TPU v7x, 256 devices: a whole 4x4x8 slice. The times are simulated.
256 devices in a mesh: rep: 2 (over z_hi), fs: 16 (over z_lo, y), tp: 8 (over x, core).
Axes of the slice: x: 4, y: 4, z: 8 (z_hi: 2, z_lo: 4; z = z_hi * 4 + z_lo), core: 2. Of those that a mesh axis runs over, the one named last changes fastest.
Arguments:
- tokens: bfloat16 [65536, 2048], P(('rep', 'fs', 'tp')), may hold values from -6 to 6
- norm_gain: float32 [2048], replicated, may hold values from 0.1 to 1.9
- gate_weight: float32 [2048, 5120], P('fs', 'tp'), may hold values from -0.125 to 0.125
- gate_scale: float32 [5120], P('tp'), may hold values from 0.1 to 1.9
- up_weight: float32 [2048, 5120], P('fs', 'tp'), may hold values from -0.125 to 0.125
- up_scale: float32 [5120], P('tp'), may hold values from 0.1 to 1.9
- down_weight: float32 [5120, 2048], P('tp', 'fs'), may hold values from -0.078125 to 0.078125
- down_scale: float32 [2048], replicated, may hold values from 0.1 to 1.9
Outputs:
- mixed: bfloat16 [65536, 2048], P(('rep', 'fs', 'tp'))
All inputs are finite; a program needn't handle non-finite values.
Results may differ from a plain program's by a relative error of at most 0.013.
Values may be sent and summed in bfloat16 or wider, within the bound.
No kernel may reach another device: no remote copies, remote signals or barrier semaphores. Data moves between devices by JAX's collectives and lax.ppermute only.
A program may use at most 128 MiB of HBM per device.

v0:
```python
import jax
import jax.numpy as jnp
from jax import lax
from jax.sharding import PartitionSpec as P

EPS_VALUE = 1e-06


def rows_first(arrays, axis, dims):
    turned = [jnp.moveaxis(a, dim, 0) for a, dim in zip(arrays, dims)]
    both = jnp.concatenate([t.reshape(len(t), -1) for t in turned], axis=1)
    whole, at, outs = (lax.all_gather(both, axis, axis=0, tiled=True), 0, [])
    for t, dim in zip(turned, dims):
        piece = whole[:, at : at + t[0].size].reshape(-1, *t.shape[1:])
        outs.append(jnp.moveaxis(piece, 0, dim))
        at += t[0].size
    return tuple(outs)


def joined_along(parts, dim):
    parts = jnp.moveaxis(parts, 0, dim)
    shape = parts.shape
    return parts.reshape(*shape[:dim], shape[dim] * shape[dim + 1], *shape[dim + 2 :])


def piecewise(shard, axis, dim, apply, out_dim):
    peers, rows = (lax.axis_size(axis), shard.shape[dim])
    count = 2 if rows % 2 == 0 else 1
    outs, length = ([], rows // count)
    for k in range(count):
        piece = lax.slice_in_dim(shard, k * length, (k + 1) * length, axis=dim)
        starts = jnp.arange(peers) * rows + k * length
        outs.append(jax.vmap(apply)(lax.all_gather(piece, axis), starts))
    return joined_along(jnp.concatenate(outs, axis=out_dim + 1), out_dim)


def normalize(token_rows, norm_gain):
    values = token_rows.astype(jnp.float32)
    inverse = lax.rsqrt(jnp.mean(values * values, axis=-1, keepdims=True) + EPS_VALUE)
    return (values * inverse * norm_gain).astype(jnp.bfloat16)


def body(tokens, norm_gain, gate_weight, gate_scale, up_weight, up_scale, down_weight, down_scale):
    normed = normalize(tokens, norm_gain)
    gate_bf = gate_weight.astype(jnp.bfloat16)
    up_bf = up_weight.astype(jnp.bfloat16)
    down_bf = down_weight.astype(jnp.bfloat16)
    gate_full, up_full, down_full = rows_first((gate_bf, up_bf, down_bf), "fs", (0, 0, 1))

    def expand(slab_rows, offset):
        gate_pre = jnp.dot(slab_rows, gate_full, preferred_element_type=jnp.float32) * gate_scale
        up_pre = jnp.dot(slab_rows, up_full, preferred_element_type=jnp.float32) * up_scale
        return (jax.nn.silu(gate_pre) * up_pre).astype(jnp.bfloat16)

    hidden = piecewise(normed, "tp", 0, expand, 0)
    partial_value = (
        jnp.dot(hidden, down_full, preferred_element_type=jnp.float32) * down_scale
    ).astype(jnp.bfloat16)
    partial_value = lax.optimization_barrier(partial_value)
    return lax.psum_scatter(
        partial_value.astype(jnp.float32).astype(jnp.bfloat16),
        "tp",
        scatter_dimension=0,
        tiled=True,
    )


def solution(mesh):
    return jax.shard_map(
        body,
        mesh=mesh,
        in_specs=(
            P(("rep", "fs", "tp"), None),
            P(),
            P("fs", "tp"),
            P("tp"),
            P("fs", "tp"),
            P("tp"),
            P("tp", "fs"),
            P(),
        ),
        out_specs=P(("rep", "fs", "tp"), None),
        check_vma=False,
    )
```

profile of v0, /device:TPU:1, one launch (start us, length us, event | category | flops | bytes accessed | tf_op | source)
XLA Modules:
  0.0 268.4 jit_solution(17899285519200331253)
XLA Ops:
  6.5 1.5 fusion.1
  8.1 1.6 fusion.3
  9.7 1.1 fusion.8
  10.8 0.0 all-gather.8.cloned.1.call-update
  10.8 0.0 all-gather.6.cloned.1.call-start
  10.9 0.2 copy.9
  11.1 0.8 pad_maximum_fusion.1
  12.0 0.0 all-gather.6.cloned.1.call-update
  12.0 0.0 all-gather.10.cloned.1.call-start
  12.0 0.7 all-gather.10.cloned.1.call-update
  12.7 0.0 reduce-scatter.2.cloned.1.call-start
  12.8 37.0 %all-gather.8.cloned.1.call-done = bf16[1024,2048]{1,0:T(8,128)(2,1)} async-done(((bf16[128,2048]{1,0:T(8,128)(2,1)}), bf16[1024,2048]{1,0:T(8,128)(2,1)}) %all-gather.8.cloned.1.call-update) | async-done | bytes 4194320 | tf_op jit(solution)/shard_map/all_gather | solution.py:33
  49.8 95.3 %all-gather.6.cloned.1.call-done = bf16[2048,1920]{1,0:T(8,128)(2,1)} async-done(((bf16[128,1920]{1,0:T(8,128)(2,1)}), bf16[2048,1920]{1,0:T(8,128)(2,1)}) %all-gather.6.cloned.1.call-update) | async-done | bytes 7864336 | tf_op jit(solution)/shard_map/all_gather | solution.py:12
  145.1 6.0 %fusion.5 = f32[8,128,640]{2,1,0:T(8,128)S(1)} fusion(bf16[8,128,2048]{2,1,0:T(8,128)(2,1)} %bitcast.25, bf16[2048,1920]{1,0:T(8,128)(2,1)} %all-gather.6.cloned.1.call-done), kind=kOutput, calls=%fused_computation.13 | convolution fusion | flops 2684354560 | bytes 9437184 | tf_op jit(solution)/shard_map/vmap()/dot_general | solution.py:51
  151.1 33.0 %all-gather.10.cloned.1.call-done = bf16[1024,2048]{1,0:T(8,128)(2,1)} async-done(((bf16[128,2048]{1,0:T(8,128)(2,1)}), bf16[1024,2048]{1,0:T(8,128)(2,1)}) %all-gather.10.cloned.1.call-update) | async-done | bytes 4194320 | tf_op jit(solution)/shard_map/all_gather | solution.py:33
  184.1 6.1 %fusion.4 = f32[8,128,640]{2,1,0:T(8,128)S(1)} fusion(bf16[8,128,2048]{2,1,0:T(8,128)(2,1)} %bitcast.27, bf16[2048,1920]{1,0:T(8,128)(2,1)} %all-gather.6.cloned.1.call-done), kind=kOutput, calls=%fused_computation.12 | convolution fusion | flops 2684354560 | bytes 9437184 | tf_op jit(solution)/shard_map/vmap()/dot_general | solution.py:51
  190.3 0.3 copy-done.4
  190.6 3.6 %multiply_convert_fusion.2 = bf16[8,128,640]{2,1,0:T(8,128)(2,1)S(1)} fusion(f32[8,128,640]{2,1,0:T(8,128)S(1)} %fusion.5, bf16[8,128,2048]{2,1,0:T(8,128)(2,1)S(1)} %bitcast.26, bf16[2048,1920]{1,0:T(8,128)(2,1)S(1)} %copy-done.3, f32[640]{0:T(1024)S(1)} %copy-done.7, f32[640]{0:T(1024)S(1)} %copy-done.8), kind=kOutput, calls=%fused_computation.8 | convolution fusion | flops 2689597440 | bytes 10756096 | tf_op jit(solution)/shard_map/vmap()/dot_general | solution.py:52
  194.2 3.6 %multiply_convert_fusion.1 = bf16[8,128,640]{2,1,0:T(8,128)(2,1)S(1)} fusion(f32[8,128,640]{2,1,0:T(8,128)S(1)} %fusion.4, bf16[8,128,2048]{2,1,0:T(8,128)(2,1)S(1)} %bitcast.28, bf16[2048,1920]{1,0:T(8,128)(2,1)S(1)} %copy-done.3, f32[640]{0:T(1024)S(1)} %copy-done.7, f32[640]{0:T(1024)S(1)} %copy-done.8), kind=kOutput, calls=%fused_computation.7 | convolution fusion | flops 2689597440 | bytes 10756096 | tf_op jit(solution)/shard_map/vmap()/dot_general | solution.py:52
  197.9 0.2 pad_maximum_fusion
  198.1 0.5 copy-done.6
  198.6 9.1 %multiply_convert_fusion = bf16[2048,2048]{1,0:T(8,128)(2,1)} fusion(bf16[2048,640]{1,0:T(8,128)(2,1)S(1)} %bitcast.23, f32[2048]{0:T(1024)S(1)} %copy-done.6, bf16[2048,1920]{1,0:T(8,128)(2,1)S(1)} %copy-done.3), kind=kOutput, calls=%fused_computation | convolution fusion | flops 5377097728 | bytes 13639680 | tf_op jit(solution)/shard_map/dot_general | solution.py:57
  207.6 0.0 reduce-scatter.2.cloned.1.call-update
  207.7 54.2 %reduce-scatter.2.cloned.1.call-done = bf16[256,2048]{1,0:T(8,128)(2,1)} async-done(((bf16[2048,2048]{1,0:T(8,128)(2,1)}), bf16[256,2048]{1,0:T(8,128)(2,1)}) %reduce-scatter.2.cloned.1.call-update) | async-done | bytes 1048592 | tf_op jit(solution)/shard_map/reduce_scatter | solution.py:60
  (20 shorter events, 0.1 us)
Async XLA Ops:
  6.5 43.2 %all-gather.8.cloned.1.call-start = ((), (), s32[]{:S(2)}) async-start(), calls=%async_computation.3 | async-start | bytes 4718592 | tf_op jit(solution)/shard_map/all_gather | solution.py:33
  8.0 2.9 %copy-start = (f32[640,128]{1,0:T(8,128)S(1)}, f32[640,128]{1,0:T(8,128)}, u32[]{:S(2)}) copy-start(f32[640,128]{1,0:T(8,128)} %param.14) | copy-start | bytes 983044
  8.1 3.0 %copy-start.1 = (f32[128,640]{1,0:T(8,128)S(1)}, f32[128,640]{1,0:T(8,128)}, u32[]{:S(2)}) copy-start(f32[128,640]{1,0:T(8,128)} %param.10) | copy-start | bytes 983044
  8.1 3.0 %copy-start.2 = (f32[128,640]{1,0:T(8,128)S(1)}, f32[128,640]{1,0:T(8,128)}, u32[]{:S(2)}) copy-start(f32[128,640]{1,0:T(8,128)} %param.12) | copy-start | bytes 983044
  10.8 134.2 %all-gather.6.cloned.1.call-start = ((), (), s32[]{:S(2)}) async-start(), calls=%async_computation.1 | async-start | bytes 8355840 | tf_op jit(solution)/shard_map/all_gather | solution.py:12
  12.0 172.1 %all-gather.10.cloned.1.call-start = ((), (), s32[]{:S(2)}) async-start(), calls=%async_computation.4 | async-start | bytes 4718592 | tf_op jit(solution)/shard_map/all_gather | solution.py:33
  12.7 249.1 %reduce-scatter.2.cloned.1.call-start = ((), (), s32[]{:S(2)}) async-start(), calls=%async_computation.2 | async-start | bytes 9437184 | tf_op jit(solution)/shard_map/reduce_scatter | solution.py:60
  184.1 6.2 %copy-start.3 = (bf16[2048,1920]{1,0:T(8,128)(2,1)S(1)}, bf16[2048,1920]{1,0:T(8,128)(2,1)}, u32[]{:S(2)}) copy-start(bf16[2048,1920]{1,0:T(8,128)(2,1)} %all-gather.6.cloned.1.call-done) | copy-start | bytes 23592964
  184.1 6.5 %copy-start.4 = (bf16[1024,2048]{1,0:T(8,128)(2,1)S(1)}, bf16[1024,2048]{1,0:T(8,128)(2,1)}, u32[]{:S(2)}) copy-start(bf16[1024,2048]{1,0:T(8,128)(2,1)} %all-gather.8.cloned.1.call-done) | copy-start | bytes 12582916
  184.1 6.5 %copy-start.7 = (f32[640]{0:T(1024)S(1)}, f32[640]{0:T(1024)}, u32[]{:S(2)}) copy-start(f32[640]{0:T(1024)} %param.13) | copy-start | bytes 7684
  184.1 6.5 %copy-start.8 = (f32[640]{0:T(1024)S(1)}, f32[640]{0:T(1024)}, u32[]{:S(2)}) copy-start(f32[640]{0:T(1024)} %param.11) | copy-start | bytes 7684
  190.6 3.6 %copy-start.5 = (bf16[1024,2048]{1,0:T(8,128)(2,1)S(1)}, bf16[1024,2048]{1,0:T(8,128)(2,1)}, u32[]{:S(2)}) copy-start(bf16[1024,2048]{1,0:T(8,128)(2,1)} %all-gather.10.cloned.1.call-done) | copy-start | bytes 12582916
  197.9 0.7 copy-start.6
Sparse Core Ops, SparseCore 0:
  11.0 38.7 all-gather.7
  51.5 93.4 all-gather.5
  146.9 37.1 all-gather.9
  207.8 54.0 reduce-scatter.1
where the time goes:
time: 269 us; the launch traced here: 268 us
  waiting for transfers between devices  220 us (82%)
  matrix products  28.5 us (11%)
  between operations  13.3 us (5%)
  other arithmetic  4.22 us (2%)
    all_gather x1, waiting for transfers between devices, rows_first(): whole, at, outs = (lax.all_gather(both, axis, axis=0, tiled=True), 0, [])  95.3 us
    all_gather x2, waiting for transfers between devices, piecewise(): outs.append(jax.vmap(apply)(lax.all_gather(piece, axis), starts))  70 us
    reduce_scatter x1, waiting for transfers between devices, body(): lax.psum_scatter(partial_value.astype(jnp.float32).astype(jnp.bfloat16),...  54.2 us
    dot_general x2, matrix products, expand(): jnp.dot(slab_rows, gate_full, preferred_element_type=jnp.float32)  12.1 us
    dot_general x1, matrix products, body(): jnp.dot(hidden, down_full, preferred_element_type=jnp.float32) * down_scale  9.07 us
    dot_general x2, matrix products, expand(): jnp.dot(slab_rows, up_full, preferred_element_type=jnp.float32) * up_scale  7.26 us
  transfers between devices with their start and end apart: 4, of which 4 were waited for; matrix products, arithmetic and copies ran while one was open for 3% of the time, Pallas kernels for 0%

commit v1 on v0

--- a/solution.py
+++ b/solution.py
@@ -9,7 +9,16 @@
 def rows_first(arrays, axis, dims):
     turned = [jnp.moveaxis(a, dim, 0) for a, dim in zip(arrays, dims)]
     both = jnp.concatenate([t.reshape(len(t), -1) for t in turned], axis=1)
-    whole, at, outs = (lax.all_gather(both, axis, axis=0, tiled=True), 0, [])
+    whole, at, outs = (
+        jnp.concatenate(
+            lax.all_to_all(
+                jnp.stack([both for _ in range(lax.axis_size(axis))], axis=0), axis, 0, 0
+            ),
+            axis=0,
+        ),
+        0,
+        [],
+    )
     for t, dim in zip(turned, dims):
         piece = whole[:, at : at + t[0].size].reshape(-1, *t.shape[1:])
         outs.append(jnp.moveaxis(piece, 0, dim))

time: 269 us -> 292 us (1.086)
  starting transfers between devices: 0.12 us -> 9.47 us
  local copies, waits for them, and re-layouts: 2.05 us -> 8.22 us
  matrix products: 28.5 us -> 33.6 us
  waiting for transfers between devices: 220 us -> 225 us
    all_to_all x0 -> x1, waiting for transfers between devices: none -> 104 us  [rows_first(): lax.all_to_all(jnp.stack([both for _ in range(lax.axis_size(axis))], axis...]
    all_gather x1 -> x0, waiting for transfers between devices: 95.3 us -> none  [rows_first(): whole, at, outs = (lax.all_gather(both, axis, axis=0, tiled=True), 0, [])]
    all_gather x2, waiting for transfers between devices: 70 us -> 35.8 us  [piecewise(): outs.append(jax.vmap(apply)(lax.all_gather(piece, axis), starts))]
    reduce_scatter x1, waiting for transfers between devices: 54.2 us -> 84.5 us  [body(): lax.psum_scatter(partial_value.astype(jnp.float32).astype(jnp.bfloat16),...]
    all_to_all x0 -> x1, starting transfers between devices: none -> 9.35 us  [rows_first(): lax.all_to_all(jnp.stack([both for _ in range(lax.axis_size(axis))], axis...]
    another operation x0 -> x1, local copies, waits for them, and re-layouts: none -> 4.1 us  [rows_first(): jnp.stack([both for _ in range(lax.axis_size(axis))], axis=0)]
    dot_general x2, matrix products: 7.26 us -> 10.8 us  [expand(): jnp.dot(slab_rows, up_full, preferred_element_type=jnp.float32) * up_scale]
  transfers between devices with their start and end apart: 4 -> 4, of which waited for: 4 -> 3; matrix products, arithmetic and copies ran while one was open for 3% -> 3% of each run, Pallas kernels for 0% -> 0%
where the time goes in v1:
time: 292 us; the launch traced here: 291 us
  waiting for transfers between devices  225 us (77%)
  matrix products  33.6 us (12%)
  between operations  13.3 us (5%)
  starting transfers between devices  9.47 us (3%)
  local copies, waits for them, and re-layouts  8.22 us (3%)
    all_to_all x1, waiting for transfers between devices, rows_first(): lax.all_to_all(jnp.stack([both for _ in range(lax.axis_size(axis))], axis...  104 us
    reduce_scatter x1, waiting for transfers between devices, body(): lax.psum_scatter(partial_value.astype(jnp.float32).astype(jnp.bfloat16),...  84.5 us
    all_gather x2, waiting for transfers between devices, piecewise(): outs.append(jax.vmap(apply)(lax.all_gather(piece, axis), starts))  35.8 us
    dot_general x2, matrix products, expand(): jnp.dot(slab_rows, gate_full, preferred_element_type=jnp.float32)  12.1 us
    dot_general x2, matrix products, expand(): jnp.dot(slab_rows, up_full, preferred_element_type=jnp.float32) * up_scale  10.8 us
    dot_general x1, matrix products, body(): jnp.dot(hidden, down_full, preferred_element_type=jnp.float32) * down_scale  10.7 us
    all_to_all x1, starting transfers between devices, rows_first(): lax.all_to_all(jnp.stack([both for _ in range(lax.axis_size(axis))], axis...  9.35 us
  transfers between devices with their start and end apart: 4, of which 3 were waited for; matrix products, arithmetic and copies ran while one was open for 3% of the time, Pallas kernels for 0%

profile of v1, /device:TPU:1, one launch (start us, length us, event | category | flops | bytes accessed | tf_op | source)
XLA Modules:
  0.0 291.3 jit_solution(13983659900307279661)
XLA Ops:
  6.5 1.0 convert_bitcast_fusion
  7.5 1.1 copy.10
  8.7 1.1 copy.9
  9.8 0.3 copy.11
  10.1 4.1 %stack.2 = bf16[16,128,1920]{2,1,0:T(8,128)(2,1)} broadcast(bf16[128,1920]{1,0:T(8,128)(2,1)S(1)} %copy.11), dimensions={1,2} | broadcast | bytes 8355840 | tf_op jit(solution)/shard_map/stack | solution.py:15
  14.2 9.3 %all-to-all-start = ((bf16[16,128,1920]{2,1,0:T(8,128)(2,1)}), bf16[16,128,1920]{2,1,0:T(8,128)(2,1)}, u32[]{:S(2)}, u32[]{:S(2)}) async-start(bf16[16,128,1920]{2,1,0:T(8,128)(2,1)} %stack.2), calls=%async_computation | async-start | bytes 15728640 | tf_op jit(solution)/shard_map/all_to_all | solution.py:14
  23.6 0.0 all-gather.5.cloned.1.call-start
  23.6 0.3 fusion.1
  23.9 0.3 fusion.3
  24.2 1.1 fusion.8
  25.4 0.0 all-gather.7.cloned.1.call-start
  25.4 0.7 all-gather.7.cloned.1.call-update
  26.1 0.0 reduce-scatter.2.cloned.1.call-start
  26.2 35.8 %all-gather.5.cloned.1.call-done = bf16[1024,2048]{1,0:T(8,128)(2,1)} async-done(((bf16[128,2048]{1,0:T(8,128)(2,1)}), bf16[1024,2048]{1,0:T(8,128)(2,1)}) %all-gather.5.cloned.1.call-update) | async-done | bytes 4194320 | tf_op jit(solution)/shard_map/all_gather | solution.py:42
  62.0 103.8 %all-to-all-done = bf16[16,128,1920]{2,1,0:T(8,128)(2,1)} async-done(((bf16[16,128,1920]{2,1,0:T(8,128)(2,1)}), bf16[16,128,1920]{2,1,0:T(8,128)(2,1)}, u32[]{:S(2)}, u32[]{:S(2)}) %all-to-all-start) | async-done | bytes 7864352 | tf_op jit(solution)/shard_map/all_to_all | solution.py:14
  165.7 6.0 %fusion.5 = f32[8,128,640]{2,1,0:T(8,128)S(1)} fusion(bf16[8,128,2048]{2,1,0:T(8,128)(2,1)} %bitcast.24, bf16[2048,1920]{1,0:T(8,128)(2,1)} %bitcast.2), kind=kOutput, calls=%fused_computation.13 | convolution fusion | flops 2684354560 | bytes 9437184 | tf_op jit(solution)/shard_map/vmap()/dot_general | solution.py:60
  171.7 0.0 all-gather.7.cloned.1.call-done
  171.8 6.1 %fusion.4 = f32[8,128,640]{2,1,0:T(8,128)S(1)} fusion(bf16[8,128,2048]{2,1,0:T(8,128)(2,1)} %bitcast.26, bf16[2048,1920]{1,0:T(8,128)(2,1)} %bitcast.2), kind=kOutput, calls=%fused_computation.12 | convolution fusion | flops 2684354560 | bytes 9437184 | tf_op jit(solution)/shard_map/vmap()/dot_general | solution.py:60
  178.0 5.5 %multiply_convert_fusion.2 = bf16[8,128,640]{2,1,0:T(8,128)(2,1)S(1)} fusion(f32[8,128,640]{2,1,0:T(8,128)S(1)} %fusion.5, bf16[8,128,2048]{2,1,0:T(8,128)(2,1)S(1)} %bitcast.25, bf16[2048,1920]{1,0:T(8,128)(2,1)} %bitcast.2, f32[640]{0:T(1024)S(1)} %copy-done.5, f32[640]{0:T(1024)S(1)} %copy-done.6), kind=kOutput, calls=%fused_computation.8 | convolution fusion | flops 2689597440 | bytes 10753024 | tf_op jit(solution)/shard_map/vmap()/dot_general | solution.py:61
  183.5 5.3 %multiply_convert_fusion.1 = bf16[8,128,640]{2,1,0:T(8,128)(2,1)S(1)} fusion(f32[8,128,640]{2,1,0:T(8,128)S(1)} %fusion.4, bf16[8,128,2048]{2,1,0:T(8,128)(2,1)S(1)} %bitcast.27, bf16[2048,1920]{1,0:T(8,128)(2,1)} %bitcast.2, f32[640]{0:T(1024)S(1)} %copy-done.5, f32[640]{0:T(1024)S(1)} %copy-done.6), kind=kOutput, calls=%fused_computation.7 | convolution fusion | flops 2689597440 | bytes 10753024 | tf_op jit(solution)/shard_map/vmap()/dot_general | solution.py:61
  188.8 0.2 pad_maximum_fusion
  189.1 0.5 copy-done.4
  189.5 10.7 %multiply_convert_fusion = bf16[2048,2048]{1,0:T(8,128)(2,1)} fusion(bf16[2048,640]{1,0:T(8,128)(2,1)S(1)} %bitcast.23, f32[2048]{0:T(1024)S(1)} %copy-done.4, bf16[2048,1920]{1,0:T(8,128)(2,1)} %bitcast.2), kind=kOutput, calls=%fused_computation | convolution fusion | flops 5377097728 | bytes 13639680 | tf_op jit(solution)/shard_map/dot_general | solution.py:66
  200.2 84.5 %reduce-scatter.2.cloned.1.call-done = bf16[256,2048]{1,0:T(8,128)(2,1)} async-done(((bf16[2048,2048]{1,0:T(8,128)(2,1)}), bf16[256,2048]{1,0:T(8,128)(2,1)}) %reduce-scatter.2.cloned.1.call-update) | async-done | bytes 1048592 | tf_op jit(solution)/shard_map/reduce_scatter | solution.py:69
  (17 shorter events, 0.1 us)
Async XLA Ops:
  14.2 9.4 %copy-start = (bf16[256,2048]{1,0:T(8,128)(2,1)S(1)}, bf16[256,2048]{1,0:T(8,128)(2,1)}, u32[]{:S(2)}) copy-start(bf16[256,2048]{1,0:T(8,128)(2,1)} %param.8) | copy-start | bytes 3145732
  14.2 9.7 %copy-start.1 = (f32[2048]{0:T(1024)S(1)}, f32[2048]{0:T(1024)}, u32[]{:S(2)}) copy-start(f32[2048]{0:T(1024)} %param.9) | copy-start | bytes 24580
  14.2 151.5 %all-to-all-start = ((bf16[16,128,1920]{2,1,0:T(8,128)(2,1)}), bf16[16,128,1920]{2,1,0:T(8,128)(2,1)}, u32[]{:S(2)}, u32[]{:S(2)}) async-start(bf16[16,128,1920]{2,1,0:T(8,128)(2,1)} %stack.2), calls=%async_computation | async-start | bytes 15728640 | tf_op jit(solution)/shard_map/all_to_all | solution.py:14
  23.6 38.4 %all-gather.5.cloned.1.call-start = ((), (), s32[]{:S(2)}) async-start(), calls=%async_computation.3 | async-start | bytes 4718592 | tf_op jit(solution)/shard_map/all_gather | solution.py:42
  25.4 146.4 %all-gather.7.cloned.1.call-start = ((), (), s32[]{:S(2)}) async-start(), calls=%async_computation.4 | async-start | bytes 4718592 | tf_op jit(solution)/shard_map/all_gather | solution.py:42
  26.1 258.6 %reduce-scatter.2.cloned.1.call-start = ((), (), s32[]{:S(2)}) async-start(), calls=%async_computation.2 | async-start | bytes 9437184 | tf_op jit(solution)/shard_map/reduce_scatter | solution.py:69
  171.8 6.2 %copy-start.2 = (bf16[1024,2048]{1,0:T(8,128)(2,1)S(1)}, bf16[1024,2048]{1,0:T(8,128)(2,1)}, u32[]{:S(2)}) copy-start(bf16[1024,2048]{1,0:T(8,128)(2,1)} %all-gather.5.cloned.1.call-done) | copy-start | bytes 12582916
  171.8 6.2 %copy-start.5 = (f32[640]{0:T(1024)S(1)}, f32[640]{0:T(1024)}, u32[]{:S(2)}) copy-start(f32[640]{0:T(1024)} %param.13) | copy-start | bytes 7684
  171.8 6.2 %copy-start.6 = (f32[640]{0:T(1024)S(1)}, f32[640]{0:T(1024)}, u32[]{:S(2)}) copy-start(f32[640]{0:T(1024)} %param.11) | copy-start | bytes 7684
  178.0 5.5 %copy-start.3 = (bf16[1024,2048]{1,0:T(8,128)(2,1)S(1)}, bf16[1024,2048]{1,0:T(8,128)(2,1)}, u32[]{:S(2)}) copy-start(bf16[1024,2048]{1,0:T(8,128)(2,1)} %all-gather.7.cloned.1.call-done) | copy-start | bytes 12582916
  188.8 0.7 copy-start.4
Sparse Core Ops, SparseCore 0:
  26.2 35.7 all-gather.4
  63.9 34.5 all-gather.6
  200.3 84.3 reduce-scatter.1
